TPU v7x, 256 devices: a whole 4x4x8 slice. The times are simulated.
256 devices in a mesh: ep: 16 (over y, x), tp: 16 (over z, core).
Axes of the slice: x: 4, y: 4, z: 8, core: 2. Of those that a mesh axis runs over, the one named last changes fastest.
Arguments:
- tokens: bfloat16 [1024, 2048], P('ep', 'tp'), may hold values from -6 to 6
- norm_gain: float32 [2048], replicated, may hold values from 0.5 to 1.5
- group_pick: int32 [1024, 1], P('ep'), may hold values from 0 to 15; in each aligned block of 64 rows (0 to 63, 64 to 127, ...) at most 18 rows name the same one
- inner_pick: int32 [1024, 2], P('ep'), may hold values from 0 to 3, all different within a row
- route_weight: float32 [1024, 2], P('ep'), may hold values from 0.3 to 1
- w_gate: bfloat16 [64, 1024, 2048], P('ep', 'tp'), may hold values from -0.125 to 0.125
- w_up: bfloat16 [64, 1024, 2048], P('ep', 'tp'), may hold values from -0.125 to 0.125
- w_down: bfloat16 [64, 1024, 2048], P('ep', 'tp'), may hold values from -0.1875 to 0.1875
Outputs:
- mixed: bfloat16 [1024, 2048], P('ep', 'tp')
Inputs may be any that keep to these rules, and one draw needn't show every extreme that they name: `group_pick`: every entry is a group, 0 to 15; among the 64 tokens of any one index of ep no group is chosen more than 18 times, a bound that some block reaches. `inner_pick`: each row names 2 different experts of the chosen group, each 0 to 3.
All inputs are finite; a program needn't handle non-finite values.
Results may differ from a plain program's by a relative error of at most 0.002.
Values may be sent and summed in bfloat16 or wider, within the bound.
A program may use at most 64 MiB of HBM per device.

v0:
```python
import jax
import jax.numpy as jnp
from jax import lax
from jax.sharding import PartitionSpec as P

epsilon = 1e-06


def scattered(portion, rows, axis):
    count = rows * lax.axis_size(axis)
    return lax.psum_scatter(portion(jnp.int32(0), count), axis, scatter_dimension=0, tiled=True)


def rms_normed(rows, norm_gain):
    widened = rows.astype(jnp.float32)
    scaled = lax.rsqrt(jnp.mean(widened * widened, axis=-1, keepdims=True) + epsilon)
    return (widened * scaled * norm_gain).astype(jnp.bfloat16)


def per_device(tokens, norm_gain, group_pick, inner_pick, route_weight, w_gate, w_up, w_down):
    ep_size = lax.axis_size("ep")
    tok_rows = tokens.shape[0]
    feature_share = tokens.shape[1]
    inner_count = w_gate.shape[0]
    capacity = min(tok_rows, 4 * tok_rows // ep_size + 2)
    slot_count = ep_size * capacity
    groups = group_pick[:, 0]
    member = (groups[:, None] == jnp.arange(ep_size, dtype=jnp.int32)[None, :]).astype(jnp.int32)
    earlier = jnp.sum((jnp.cumsum(member, axis=0) - member) * member, axis=1)
    position = (groups * capacity + earlier).astype(jnp.int32)
    placing = position[None, :] == jnp.arange(slot_count, dtype=jnp.int32)[:, None]
    local_gates = jnp.sum(
        jax.nn.one_hot(inner_pick, inner_count, dtype=jnp.float32) * route_weight[:, :, None],
        axis=1,
    )
    packed_rows = jnp.dot(
        placing.astype(jnp.bfloat16), tokens, preferred_element_type=jnp.float32
    ).astype(jnp.bfloat16)
    packed_gates = jnp.dot(
        placing.astype(jnp.float32), local_gates, precision=lax.Precision.HIGHEST
    )
    packed_rows = packed_rows.reshape(ep_size, capacity, feature_share)
    packed_gates = packed_gates.reshape(ep_size, capacity, inner_count)
    arrived_rows = lax.all_to_all(packed_rows, "ep", split_axis=0, concat_axis=0, tiled=True)
    arrived_gates = lax.all_to_all(packed_gates, "ep", split_axis=0, concat_axis=0, tiled=True)
    full_rows = lax.all_gather(arrived_rows, "tp", axis=2, tiled=True).reshape(slot_count, -1)
    normed = rms_normed(full_rows, norm_gain)
    gate_proj = jnp.einsum("sd,efd->esf", normed, w_gate, preferred_element_type=jnp.float32)
    up_proj = jnp.einsum("sd,efd->esf", normed, w_up, preferred_element_type=jnp.float32)
    hidden = (jax.nn.silu(gate_proj) * up_proj).astype(jnp.bfloat16)
    slot_gates = jnp.transpose(arrived_gates.reshape(slot_count, inner_count))

    def weighted_sum(down_part):
        products = jnp.einsum("esf,efd->esd", hidden, down_part, preferred_element_type=jnp.float32)
        return jnp.sum(slot_gates[:, :, None] * products, axis=0)

    def column_term(first_row, row_count):
        down_part = lax.dynamic_slice_in_dim(w_down, first_row, row_count, 2)
        return jnp.transpose(weighted_sum(down_part))

    own_share = scattered(column_term, feature_share, "tp")
    partial_rows = jnp.transpose(own_share).reshape(ep_size, capacity, feature_share)
    returned = (
        lax.all_to_all(
            partial_rows.astype(jnp.bfloat16), "ep", split_axis=0, concat_axis=0, tiled=True
        )
        .astype(partial_rows.dtype)
        .reshape(slot_count, feature_share)
    )
    mixed_rows = jnp.take(returned, position, axis=0)
    return mixed_rows.astype(jnp.bfloat16)


def solution(mesh):
    return jax.shard_map(
        per_device,
        mesh=mesh,
        in_specs=(
            P("ep", "tp"),
            P(),
            P("ep", None),
            P("ep", None),
            P("ep", None),
            P("ep", "tp", None),
            P("ep", "tp", None),
            P("ep", "tp", None),
        ),
        out_specs=P("ep", "tp"),
        check_vma=False,
    )
```

profile of v0, /device:TPU:2, one launch (start us, length us, event | category | flops | bytes accessed | tf_op | source)
XLA Modules:
  0.0 157.6 jit_solution(5394190780620000471)
XLA Ops:
  6.5 0.0 copy-start
  6.5 0.0 all-gather.2.cloned.1.call-start
  6.5 0.8 fusion.14
  7.4 0.1 reduce_window_sum.11
  7.5 0.8 select_reduce_fusion
  8.3 0.7 multiply_add_fusion.1
  9.0 0.9 convolution_convert_fusion
  9.9 13.8 %all_to_all.15 = bf16[16,18,128]{2,1,0:T(8,128)(2,1)} all-to-all(bf16[16,18,128]{2,1,0:T(8,128)(2,1)S(1)} %reshape.69), channel_id=1, replica_groups=mesh['ep'=16,'tp'=16] {'ep'}, dimensions={0} | all-to-all | bytes 147456 | tf_op jit(solution)/shard_map/all_to_all | solution.py:44
  23.7 0.0 all-gather.2.cloned.1.call-update
  23.7 0.0 reduce-scatter.2.cloned.1.call-start
  23.8 0.7 select_reduce_fusion.1
  24.5 0.6 fusion.9
  25.1 10.7 %all_to_all.16 = f32[16,18,4]{1,2,0:T(4,128)S(1)} all-to-all(f32[16,18,4]{1,2,0:T(4,128)S(1)} %fusion.9), channel_id=1, replica_groups=mesh['ep'=16,'tp'=16] {'ep'}, dimensions={0} | all-to-all | bytes 9216 | tf_op jit(solution)/shard_map/all_to_all | solution.py:45
  35.9 0.1 reshape.68
  36.0 26.9 %all-gather.2.cloned.1.call-done = bf16[16,18,2048]{2,1,0:T(8,128)(2,1)} async-done(((bf16[16,18,128]{2,1,0:T(8,128)(2,1)}), bf16[16,18,2048]{2,1,0:T(8,128)(2,1)}) %all-gather.2.cloned.1.call-update) | async-done | bytes 1179664 | tf_op jit(solution)/shard_map/all_gather | solution.py:46
  62.9 1.8 %multiply_reduce_fusion.1 = f32[16,18]{1,0:T(8,128)S(1)} fusion(bf16[16,18,2048]{2,1,0:T(8,128)(2,1)} %all-gather.2.cloned.1.call-done), kind=kLoop, calls=%fused_computation.2 | loop fusion | flops 1769184 | bytes 1180800 | tf_op jit(solution)/shard_map/reduce_sum | solution.py:16
  64.7 0.0 copy-start.1
  64.7 0.1 rsqrt.12
  64.8 1.5 reshape.72
  66.4 0.0 copy-done.1
  66.4 2.8 %convolution_bitcast_fusion.1 = f32[4,288,64]{1,2,0:T(8,128)} fusion(bf16[4,64,2048]{2,1,0:T(8,128)(2,1)} %param.13, f32[288,2048]{1,0:T(8,128)S(1)} %reshape.72, f32[2048]{0:T(1024)S(1)} %copy-done.1, f32[288]{0:T(512)S(1)} %rsqrt.12), kind=kOutput, calls=%fused_computation.6 | convolution fusion | flops 303759360 | bytes 3712128 | tf_op jit(solution)/shard_map/sd,efd->esf/dot_general | solution.py:48
  69.1 0.0 copy-done
  69.1 5.3 %multiply_reduce_fusion = f32[288,2048]{1,0:T(8,128)} fusion(f32[4,288]{1,0:T(4,128)S(1)} %bitcast.39, bf16[4,64,2048]{2,1,0:T(8,128)(2,1)S(1)} %copy-done, bf16[4,64,2048]{2,1,0:T(8,128)(2,1)} %param.14, f32[4,288,64]{1,2,0:T(8,128)} %convolution_bitcast_fusion.1, f32[288,2048]{1,0:T(8,128)S(1)} %reshape.72, f32[2048]{0:T(1024)S(1)} %copy-done.1, ...), kind=kOutput, calls=%fused_computation.1 | convolution fusion | flops 610320384 | bytes 7124608 | tf_op jit(solution)/shard_map/esf,efd->esd/dot_general | solution.py:54
  74.4 0.0 reduce-scatter.2.cloned.1.call-update
  74.4 0.6 copy-done.2
  75.1 59.0 %reduce-scatter.2.cloned.1.call-done = f32[128,288]{0,1:T(8,128)} async-done(((f32[2048,288]{0,1:T(8,128)}), f32[128,288]{0,1:T(8,128)}) %reduce-scatter.2.cloned.1.call-update) | async-done | bytes 147472 | tf_op jit(solution)/shard_map/reduce_scatter | solution.py:11
  134.1 0.9 convert_bitcast_fusion
  135.0 0.6 convert_element_type.47
  135.7 7.3 %all-to-all-start.2 = ((bf16[16,18,128]{2,1,0:T(8,128)(2,1)}), bf16[16,18,128]{2,1,0:T(8,128)(2,1)S(1)}, u32[]{:S(2)}, u32[]{:S(2)}) async-start(bf16[16,18,128]{2,1,0:T(8,128)(2,1)} %convert_element_type.47), calls=%async_computation.3 | async-start | bytes 196608 | tf_op jit(solution)/shard_map/all_to_all | solution.py:64
  143.0 6.4 %all-to-all-done.2 = bf16[16,18,128]{2,1,0:T(8,128)(2,1)S(1)} async-done(((bf16[16,18,128]{2,1,0:T(8,128)(2,1)}), bf16[16,18,128]{2,1,0:T(8,128)(2,1)S(1)}, u32[]{:S(2)}, u32[]{:S(2)}) %all-to-all-start.2) | async-done | bytes 73760 | tf_op jit(solution)/shard_map/all_to_all | solution.py:64
  149.4 0.6 gather_fusion
  150.1 0.7 select_convert_fusion
  (8 shorter events, 0.1 us)
Async XLA Ops:
  6.5 62.6 %copy-start = (bf16[4,64,2048]{2,1,0:T(8,128)(2,1)S(1)}, bf16[4,64,2048]{2,1,0:T(8,128)(2,1)}, u32[]{:S(2)}) copy-start(bf16[4,64,2048]{2,1,0:T(8,128)(2,1)} %param.15) | copy-start | bytes 3145732
  6.5 56.3 %all-gather.2.cloned.1.call-start = ((), (), s32[]{:S(2)}) async-start(), calls=%async_computation.4 | async-start | bytes 1671168 | tf_op jit(solution)/shard_map/all_gather | solution.py:46
  23.7 110.4 %reduce-scatter.2.cloned.1.call-start = ((), (), s32[]{:S(2)}) async-start(), calls=%async_computation.5 | async-start | bytes 2506752 | tf_op jit(solution)/shard_map/reduce_scatter | solution.py:11
  64.7 1.7 %copy-start.1 = (f32[2048]{0:T(1024)S(1)}, f32[2048]{0:T(1024)}, u32[]{:S(2)}) copy-start(f32[2048]{0:T(1024)} %param.9) | copy-start | bytes 24580
  74.4 0.7 copy-start.2
  135.7 13.7 %all-to-all-start.2 = ((bf16[16,18,128]{2,1,0:T(8,128)(2,1)}), bf16[16,18,128]{2,1,0:T(8,128)(2,1)S(1)}, u32[]{:S(2)}, u32[]{:S(2)}) async-start(bf16[16,18,128]{2,1,0:T(8,128)(2,1)} %convert_element_type.47), calls=%async_computation.3 | async-start | bytes 196608 | tf_op jit(solution)/shard_map/all_to_all | solution.py:64
Sparse Core Ops, SparseCore 0:
  23.8 38.9 all-gather.1
  74.6 59.5 reduce-scatter.1
where the time goes:
time: 158 us
  waiting for transfers between devices  92.4 us (58%)
  blocking collectives  24.6 us (16%)
  between operations  13.5 us (9%)
  matrix products  9.57 us (6%)
  starting transfers between devices  7.31 us (5%)
  other arithmetic  6.58 us (4%)
  local copies, waits for them, and re-layouts  3.72 us (2%)
    reduce_scatter x1, waiting for transfers between devices, scattered(): lax.psum_scatter(portion(jnp.int32(0), count), axis, scatter_dimension=0,...  59 us
    all_gather x1, waiting for transfers between devices, per_device(): lax.all_gather(arrived_rows, 'tp', axis=2, tiled=True)  26.9 us
    all_to_all x1, blocking collectives, per_device(): lax.all_to_all(packed_rows, 'ep', split_axis=0, concat_axis=0, tiled=True)  13.8 us
    all_to_all x1, blocking collectives, per_device(): lax.all_to_all(packed_gates, 'ep', split_axis=0, concat_axis=0, tiled=True)  10.7 us
    all_to_all x1, starting transfers between devices, per_device(): lax.all_to_all(partial_rows.astype(jnp.bfloat16), 'ep', split_axis=0, con...  7.26 us
    all_to_all x1, waiting for transfers between devices, per_device(): lax.all_to_all(partial_rows.astype(jnp.bfloat16), 'ep', split_axis=0, con...  6.45 us
    dot_general x1, matrix products, weighted_sum(): jnp.einsum('esf,efd->esd', hidden, down_part, preferred_element_type=jnp....  5.27 us
  transfers between devices with their start and end apart: 3, of which 3 were waited for; matrix products, arithmetic and copies ran while one was open for 1% of the time, Pallas kernels for 0%

commit v1 on v0

v1 whole, which is shorter than its diff:
```python
import functools

import jax
import jax.numpy as jnp
from jax import lax
from jax.experimental import pallas as pl
from jax.experimental.pallas import tpu as pltpu
from jax.sharding import PartitionSpec as P

MESH = pl.DeviceIdType.MESH
EPS = 1e-06
EP = 16
SIDE = 4
TP = 16
RING = 8
SLOTS = 18
PAD = 32
ROWS = EP * SLOTS
HALF = ROWS // 2
LANES = 128
F32 = jnp.float32
BF16 = jnp.bfloat16


def iota(shape, dim):
    return lax.broadcasted_iota(jnp.int32, shape, dim)


def one_hot(mask):
    return jnp.where(mask, 1.0, 0.0).astype(BF16)


def dot(a, b, dims=((1,), (0,))):
    return lax.dot_general(a, b, (dims, ((), ())), preferred_element_type=F32)


NT = ((1,), (1,))
TN = ((0,), (0,))


def kernel(
    tokens_ref, gain_ref, group_ref, inner_ref, weight_ref, w_gate_ref, w_up_ref, w_down_ref,
    out_ref,
    wgu_ref, wd_ref, place_ref, send_ref, recv_ref, tr_ref, gates_ref, x_ref, normed_ref, hl_ref,
    own_ref, give_ref, take_ref, sp_ref, sm_ref, rp_ref, rm_ref, back_ref, home_ref,
    w_sem, d_send, d_recv, agp_send, agp_recv, agm_send, agm_recv, agx_send, agx_recv,
    rx_send, rx_recv, rp_send, rp_recv, rm_send, rm_recv, h_send, h_recv,
):
    ep = lax.axis_index("ep")
    tp = lax.axis_index("tp")
    ey, ex = ep // SIDE, ep % SIDE
    z, core = tp // 2, tp % 2
    up = (tp + 2) % TP
    down = (tp + TP - 2) % TP
    partner = z * 2 + (1 - core)
    steps = [(dy, dx) for dy in range(SIDE) for dx in range(SIDE) if dy or dx]
    steps.sort(key=lambda s: -(min(s[0], SIDE - s[0]) + min(s[1], SIDE - s[1])))

    def peer(dy, dx):
        return ((ey + dy) % SIDE) * SIDE + (ex + dx) % SIDE

    barrier = pltpu.get_barrier_semaphore()
    for dy, dx in steps:
        pl.semaphore_signal(barrier, inc=1, device_id={"ep": peer(dy, dx)}, device_id_type=MESH)
    for to in (up, down, partner):
        pl.semaphore_signal(barrier, inc=1, device_id={"tp": to}, device_id_type=MESH)

    experts = w_gate_ref.shape[0]
    loads = [
        pltpu.make_async_copy(w_gate_ref, wgu_ref.at[pl.ds(0, experts)], w_sem.at[0]),
        pltpu.make_async_copy(w_up_ref, wgu_ref.at[pl.ds(experts, experts)], w_sem.at[1]),
        pltpu.make_async_copy(w_down_ref, wd_ref, w_sem.at[2]),
    ]
    for load in loads:
        load.start()

    toks = tokens_ref.shape[0]
    groups = group_ref[...]
    member = one_hot(iota((EP, toks), 0) == groups)
    before = one_hot(iota((toks, toks), 0) < iota((toks, toks), 1))
    earlier = dot(member, before)
    earlier = jnp.sum(earlier * member.astype(F32), axis=0, keepdims=True)
    position = groups * PAD + earlier.astype(jnp.int32)
    place_ref[...] = one_hot(iota((EP * PAD, toks), 0) == position)
    placing = place_ref[...]
    packed = dot(placing, tokens_ref[...]).reshape(EP, PAD, LANES)
    row = iota((16, toks), 0)
    expert = jnp.where(row >= 5, 1, 0) + jnp.where(row >= 8, 1, 0) + jnp.where(row >= 11, 1, 0)
    part = row - 2 - 3 * expert
    gate = jnp.where(inner_ref[0:1, :] == expert, weight_ref[0:1, :], 0.0) + jnp.where(
        inner_ref[1:2, :] == expert, weight_ref[1:2, :], 0.0
    )
    first = gate.astype(BF16).astype(F32)
    second = (gate - first).astype(BF16).astype(F32)
    third = gate - first - second
    parts = jnp.where(part == 0, first, jnp.where(part == 1, second, third))
    parts = jnp.where((row >= 2) & (row < 14), parts, 0.0).astype(BF16)
    parts = dot(parts, placing, NT)
    for g in range(EP):
        col = (g * PAD) // LANES * LANES
        send_ref[g, 0:16] = packed[g, 0:16].astype(BF16)
        send_ref[g, 16:32] = (packed[g, 16:32] + parts[:, col : col + LANES]).astype(BF16)

    pl.semaphore_wait(barrier, len(steps) + 3)

    sends = []
    for i, (dy, dx) in enumerate(steps):
        to = peer(dy, dx)
        sends.append(
            pltpu.make_async_remote_copy(
                send_ref.at[to], recv_ref.at[ep], d_send.at[i], d_recv.at[i],
                device_id={"ep": to}, device_id_type=MESH,
            )
        )
        sends[-1].start()
    recv_ref[ep] = send_ref[ep]
    for copy in reversed(sends):
        copy.wait_recv()

    r_col = iota((ROWS, 1), 0)
    src_col = (r_col * 3641) >> 16
    slot_col = r_col - src_col * SLOTS
    pick = one_hot(iota((ROWS, EP * PAD), 1) == src_col * PAD + slot_col)
    x_ref[tp] = dot(pick, recv_ref[...].reshape(EP * PAD, LANES)).astype(BF16)

    def ring(buf_at, send, recv, to):
        return pltpu.make_async_remote_copy(
            buf_at, buf_at, send, recv, device_id={"tp": to}, device_id_type=MESH
        )

    def piece(z_of, of_core, half):
        at = x_ref.at[z_of * 2 + of_core]
        if half is not None:
            at = at.at[pl.ds(half * HALF, HALF)]
        return at

    gp, gm, gx = [], [], []
    for i, half in enumerate((0, 1)):
        gp.append(ring(piece(z, core, half), agp_send.at[i], agp_recv.at[i], up))
        gp[-1].start()
        gm.append(ring(piece(z, core, 1 - half), agm_send.at[i], agm_recv.at[i], down))
        gm[-1].start()
    gx.append(ring(piece(z, core, None), agx_send.at[0], agx_recv.at[0], partner))
    gx[-1].start()

    tr_ref[...] = jnp.transpose(recv_ref[:, 16:32, :].astype(F32).reshape(EP * 16, LANES))
    near = tr_ref[pl.ds(pl.multiple_of((ep % 4) * PAD, PAD), PAD), :].astype(BF16)
    chosen = dot(one_hot(iota((ROWS, PAD), 1) == slot_col), near)
    lane = iota((ROWS, EP * 16), 1)
    chosen = jnp.where(lane >> 4 == src_col, chosen, 0.0).astype(BF16)
    units = w_gate_ref.shape[1]
    which = iota((EP * 16, experts * units), 0) & 15
    owner = iota((EP * 16, experts * units), 1) >> 6
    spread = one_hot((which >= 2 + 3 * owner) & (which < 5 + 3 * owner))
    gates_ref[...] = dot(chosen, spread)

    def squares(t, half):
        if half is None:
            v = x_ref[t].astype(F32)
        else:
            v = x_ref[t, half * HALF : (half + 1) * HALF].astype(F32)
        return v * v

    total = squares(tp, None)
    own_ref[0] = total
    for s in range(4):
        for i in range(2 if s < 3 else 1):
            for sign, copies, send, recv, to in (
                (-1, gp, agp_send, agp_recv, up),
                (1, gm, agm_send, agm_recv, down),
            ):
                half = i if sign < 0 else 1 - i
                z_of = (z + sign * (1 + s) + RING) % RING
                k = 2 * s + i
                ring(piece(z_of, core, half), send.at[k], recv.at[k], to).wait_recv()
                if s < 2 or (s == 2 and i == 0):
                    copies.append(ring(piece(z_of, core, half), send.at[k + 2], recv.at[k + 2], to))
                    copies[-1].start()
                n = len(gx)
                gx.append(ring(piece(z_of, core, half), agx_send.at[n], agx_recv.at[n], partner))
                gx[-1].start()
                at = pl.ds(half * HALF, HALF)
                own_ref[0, at] = own_ref[0, at] + squares(z_of * 2 + core, half)
    for copy in gx:
        copy.wait_recv()
    total = own_ref[0]
    for zz in range(RING):
        total = total + squares(zz * 2 + (1 - core), None)
    scale = lax.rsqrt(jnp.sum(total, axis=1, keepdims=True) * (1.0 / (TP * LANES)) + EPS)
    for t in range(TP):
        cols = slice(t * LANES, (t + 1) * LANES)
        normed_ref[:, cols] = (x_ref[t].astype(F32) * scale * gain_ref[:, cols]).astype(BF16)

    for load in loads:
        load.wait()
    width = experts * units
    proj = dot(normed_ref[...], wgu_ref[...].reshape(2 * width, TP * LANES), NT)
    gate_proj, up_proj = proj[:, :width], proj[:, width:]
    hidden = (gate_proj / (1.0 + jnp.exp(-gate_proj)) * up_proj).astype(BF16).astype(F32)
    gated = hidden * gates_ref[...]
    high = gated.astype(BF16)
    hl_ref[0] = high
    hl_ref[1] = (gated - high.astype(F32)).astype(BF16)

    rx = []

    def partial(offset):
        k = len(rx)
        z_of = (z + offset + RING) % RING
        cols = pl.ds(pl.multiple_of(z_of * 2 * LANES, 2 * LANES), 2 * LANES)
        w = wd_ref[:, :, cols].reshape(width, 2 * LANES)
        both = dot(hl_ref[0], w) + dot(hl_ref[1], w)
        own_ref[k] = jnp.where(core == 0, both[:, :LANES], both[:, LANES:])
        give_ref[k] = jnp.where(core == 0, both[:, LANES:], both[:, :LANES])
        rx.append(
            pltpu.make_async_remote_copy(
                give_ref.at[k], take_ref.at[k], rx_send.at[k], rx_recv.at[k],
                device_id={"tp": partner}, device_id_type=MESH,
            )
        )
        rx[-1].start()

    def mine(k, half):
        at = slice(half * HALF, (half + 1) * HALF)
        return own_ref[k, at] + take_ref[k, at]

    sp, sm = {}, {}

    def pass_on(copies, k, value, src, dst, send, recv, to):
        src[k] = value
        copies[k] = pltpu.make_async_remote_copy(
            src.at[k], dst.at[k], send.at[k], recv.at[k], device_id={"tp": to}, device_id_type=MESH
        )
        copies[k].start()

    def pass_up(k, value):
        pass_on(sp, k, value, sp_ref, rp_ref, rp_send, rp_recv, up)

    def pass_down(k, value):
        pass_on(sm, k, value, sm_ref, rm_ref, rm_send, rm_recv, down)

    partial(4)
    partial(3)
    partial(-3)
    rx[0].wait_recv()
    pass_up(0, mine(0, 0))
    pass_down(0, mine(0, 1))
    rx[1].wait_recv()
    pass_up(1, mine(1, 1))
    rx[2].wait_recv()
    pass_down(1, mine(2, 0))
    partial(2)
    partial(-2)
    sp[0].wait_recv()
    pass_up(2, mine(1, 0) + rp_ref[0])
    sm[0].wait_recv()
    pass_down(2, mine(2, 1) + rm_ref[0])
    partial(1)
    partial(-1)
    partial(0)
    rx[3].wait_recv()
    sp[1].wait_recv()
    pass_up(3, mine(3, 1) + rp_ref[1])
    rx[4].wait_recv()
    sm[1].wait_recv()
    pass_down(3, mine(4, 0) + rm_ref[1])
    sp[2].wait_recv()
    pass_up(4, mine(3, 0) + rp_ref[2])
    sm[2].wait_recv()
    pass_down(4, mine(4, 1) + rm_ref[2])
    rx[5].wait_recv()
    sp[3].wait_recv()
    pass_up(5, mine(5, 1) + rp_ref[3])
    rx[6].wait_recv()
    sm[3].wait_recv()
    pass_down(5, mine(6, 0) + rm_ref[3])
    sp[4].wait_recv()
    pass_up(6, mine(5, 0) + rp_ref[4])
    sm[4].wait_recv()
    pass_down(6, mine(6, 1) + rm_ref[4])
    rx[7].wait_recv()
    sp[5].wait_recv()
    sm[5].wait_recv()
    sp[6].wait_recv()
    sm[6].wait_recv()
    upper = mine(7, 0) + rp_ref[6] + rm_ref[5]
    lower = mine(7, 1) + rp_ref[5] + rm_ref[6]

    r_row = iota((1, ROWS), 1)
    src_row = (r_row * 3641) >> 16
    target = src_row * PAD + (r_row - src_row * SLOTS)
    unpick = one_hot(iota((EP * PAD, ROWS), 0) == target)
    summed = jnp.concatenate([upper, lower], axis=0).astype(BF16)
    back_ref[...] = dot(unpick, summed).astype(BF16).reshape(EP, PAD, LANES)
    returns = []
    for i, (dy, dx) in enumerate(steps):
        to = peer(dy, dx)
        returns.append(
            pltpu.make_async_remote_copy(
                back_ref.at[to], home_ref.at[ep], h_send.at[i], h_recv.at[i],
                device_id={"ep": to}, device_id_type=MESH,
            )
        )
        returns[-1].start()
    home_ref[ep] = back_ref[ep]
    for copy in reversed(returns):
        copy.wait_recv()
    home = home_ref[...].reshape(EP * PAD, LANES)
    out_ref[...] = dot(place_ref[...], home, TN).astype(BF16)

    for copy in sends + gp + gm + gx + rx + list(sp.values()) + list(sm.values()) + returns:
        copy.wait_send()


def per_device(tokens, norm_gain, group_pick, inner_pick, route_weight, w_gate, w_up, w_down):
    toks = tokens.shape[0]
    experts, units, model = w_gate.shape
    width = experts * units
    vmem = pl.BlockSpec(memory_space=pltpu.VMEM)
    hbm = pl.BlockSpec(memory_space=pl.ANY)
    dma = pltpu.SemaphoreType.DMA
    return pl.pallas_call(
        kernel,
        name="moe_step",
        out_shape=jax.ShapeDtypeStruct(tokens.shape, BF16),
        in_specs=[vmem] * 5 + [hbm] * 3,
        out_specs=vmem,
        scratch_shapes=[
            pltpu.VMEM((2 * experts, units, model), BF16),
            pltpu.VMEM((experts, units, model), BF16),
            pltpu.VMEM((EP * PAD, toks), BF16),
            pltpu.VMEM((EP, PAD, LANES), BF16),
            pltpu.VMEM((EP, PAD, LANES), BF16),
            pltpu.VMEM((LANES, EP * 16), F32),
            pltpu.VMEM((ROWS, width), F32),
            pltpu.VMEM((TP, ROWS, LANES), BF16),
            pltpu.VMEM((ROWS, model), BF16),
            pltpu.VMEM((2, ROWS, width), BF16),
            pltpu.VMEM((8, ROWS, LANES), F32),
            pltpu.VMEM((8, ROWS, LANES), F32),
            pltpu.VMEM((8, ROWS, LANES), F32),
            pltpu.VMEM((7, HALF, LANES), F32),
            pltpu.VMEM((7, HALF, LANES), F32),
            pltpu.VMEM((7, HALF, LANES), F32),
            pltpu.VMEM((7, HALF, LANES), F32),
            pltpu.VMEM((EP, PAD, LANES), BF16),
            pltpu.VMEM((EP, PAD, LANES), BF16),
            dma((3,)),
            dma((15,)), dma((15,)),
            dma((7,)), dma((7,)), dma((7,)), dma((7,)),
            dma((15,)), dma((15,)),
            dma((8,)), dma((8,)),
            dma((7,)), dma((7,)), dma((7,)), dma((7,)),
            dma((15,)), dma((15,)),
        ],
        compiler_params=pltpu.CompilerParams(
            collective_id=0, has_side_effects=True, vmem_limit_bytes=48 * 1024 * 1024
        ),
    )(
        tokens, norm_gain.reshape(1, model), group_pick.T, inner_pick.T, route_weight.T,
        w_gate, w_up, w_down,
    )


def solution(mesh):
    return jax.shard_map(
        per_device,
        mesh=mesh,
        in_specs=(
            P("ep", "tp"),
            P(),
            P("ep", None),
            P("ep", None),
            P("ep", None),
            P("ep", "tp", None),
            P("ep", "tp", None),
            P("ep", "tp", None),
        ),
        out_specs=P("ep", "tp"),
        check_vma=False,
    )
```

time: 158 us -> 60.1 us (0.38)
  the two profiles are of different devices: /device:TPU:2 before, /device:TPU:32 now
where the time goes in v1:
time: 60.1 us; the launch traced here: 59.8 us
  Pallas kernels  53.4 us (89%)
  local copies, waits for them, and re-layouts  6.39 us (11%)
    pallas_call x1, Pallas kernels, per_device(): pl.pallas_call(kernel, name='moe_step', out_shape=jax.ShapeDtypeStruct(to...  53.4 us
    unnamed x17, local copies, waits for them, and re-layouts  6.39 us

profile of v1, /device:TPU:32, one launch (start us, length us, event | category | flops | bytes accessed | tf_op | source)
XLA Modules:
  0.0 59.8 jit_solution(3183805293635518348)
XLA Ops:
  0.0 0.0 copy-start.6
  0.0 0.0 copy-start.5
  0.0 0.0 copy-start.7
  0.0 0.7 %copy-done.6 = f32[64,2]{0,1:T(2,128)S(1)} copy-done((f32[64,2]{0,1:T(2,128)S(1)}, f32[64,2]{0,1:T(2,128)}, u32[]{:S(2)}) %copy-start.6) | copy-done | bytes 536
  0.7 0.0 copy-done.5
  0.7 0.0 copy-done.7
  0.7 0.0 copy-start
  0.7 1.2 %copy-done = bf16[4,64,2048]{2,1,0:T(8,128)(2,1)S(1)} copy-done((bf16[4,64,2048]{2,1,0:T(8,128)(2,1)S(1)}, bf16[4,64,2048]{2,1,0:T(8,128)(2,1)}, u32[]{:S(2)}) %copy-start) | copy-done | bytes 1048600
  1.9 0.0 copy-start.1
  1.9 1.2 %copy-done.1 = bf16[4,64,2048]{2,1,0:T(8,128)(2,1)S(1)} copy-done((bf16[4,64,2048]{2,1,0:T(8,128)(2,1)S(1)}, bf16[4,64,2048]{2,1,0:T(8,128)(2,1)}, u32[]{:S(2)}) %copy-start.1) | copy-done | bytes 1048600
  3.1 0.0 copy-start.2
  3.2 1.2 %copy-done.2 = bf16[4,64,2048]{2,1,0:T(8,128)(2,1)S(1)} copy-done((bf16[4,64,2048]{2,1,0:T(8,128)(2,1)S(1)}, bf16[4,64,2048]{2,1,0:T(8,128)(2,1)}, u32[]{:S(2)}) %copy-start.2) | copy-done | bytes 1048600
  4.4 0.0 copy-start.3
  4.4 0.7 %copy-done.3 = bf16[64,128]{1,0:T(8,128)(2,1)S(1)} copy-done((bf16[64,128]{1,0:T(8,128)(2,1)S(1)}, bf16[64,128]{1,0:T(8,128)(2,1)}, u32[]{:S(2)}) %copy-start.3) | copy-done | bytes 16408
  5.1 0.0 copy-start.4
  5.1 0.7 %copy-done.4 = f32[2048]{0:T(1024)S(1)} copy-done((f32[2048]{0:T(1024)S(1)}, f32[2048]{0:T(1024)}, u32[]{:S(2)}) %copy-start.4) | copy-done | bytes 8216
  5.8 53.4 %moe_step.1 = bf16[64,128]{1,0:T(8,128)(2,1)S(1)} custom-call(bf16[64,128]{1,0:T(8,128)(2,1)S(1)} %copy-done.3, f32[1,2048]{1,0:T(1,128)S(1)} %bitcast.4, s32[1,64]{1,0:T(1,128)S(1)} %bitcast.7, s32[2,64]{1,0:T(2,128)S(1)} %bitcast.5, f32[2,64]{1,0:T(2,128)S(1)} %bitcast.6, bf16[4,64,2048]{2,1,0:T(8,128)(2,1)S(1)} %copy-done, ...), custom_call_target="tpu_custom_call" | custom-call | tf_op jit(solution)/shard_map/moe_step/pallas_call | solution.py:322
  59.2 0.6 %copy.10 = bf16[64,128]{1,0:T(8,128)(2,1)} copy(bf16[64,128]{1,0:T(8,128)(2,1)S(1)} %moe_step.1) | data formatting | bytes 32768
Async XLA Ops:
  0.0 0.7 %copy-start.6 = (f32[64,2]{0,1:T(2,128)S(1)}, f32[64,2]{0,1:T(2,128)}, u32[]{:S(2)}) copy-start(f32[64,2]{0,1:T(2,128)} %param.12) | copy-start | bytes 1540
  0.0 0.7 %copy-start.5 = (s32[64,2]{0,1:T(2,128)S(1)}, s32[64,2]{0,1:T(2,128)}, u32[]{:S(2)}) copy-start(s32[64,2]{0,1:T(2,128)} %param.11) | copy-start | bytes 1540
  0.0 0.7 %copy-start.7 = (s32[64,1]{0,1:T(1,128)S(1)}, s32[64,1]{0,1:T(1,128)}, u32[]{:S(2)}) copy-start(s32[64,1]{0,1:T(1,128)} %param.10) | copy-start | bytes 772
  0.7 1.2 %copy-start = (bf16[4,64,2048]{2,1,0:T(8,128)(2,1)S(1)}, bf16[4,64,2048]{2,1,0:T(8,128)(2,1)}, u32[]{:S(2)}) copy-start(bf16[4,64,2048]{2,1,0:T(8,128)(2,1)} %w_gate_ref.1) | copy-start | bytes 3145732
  1.9 1.2 %copy-start.1 = (bf16[4,64,2048]{2,1,0:T(8,128)(2,1)S(1)}, bf16[4,64,2048]{2,1,0:T(8,128)(2,1)}, u32[]{:S(2)}) copy-start(bf16[4,64,2048]{2,1,0:T(8,128)(2,1)} %w_up_ref.1) | copy-start | bytes 3145732
  3.1 1.2 %copy-start.2 = (bf16[4,64,2048]{2,1,0:T(8,128)(2,1)S(1)}, bf16[4,64,2048]{2,1,0:T(8,128)(2,1)}, u32[]{:S(2)}) copy-start(bf16[4,64,2048]{2,1,0:T(8,128)(2,1)} %w_down_ref.1) | copy-start | bytes 3145732
  4.4 0.7 %copy-start.3 = (bf16[64,128]{1,0:T(8,128)(2,1)S(1)}, bf16[64,128]{1,0:T(8,128)(2,1)}, u32[]{:S(2)}) copy-start(bf16[64,128]{1,0:T(8,128)(2,1)} %tokens_ref.1) | copy-start | bytes 49156
  5.1 0.7 %copy-start.4 = (f32[2048]{0:T(1024)S(1)}, f32[2048]{0:T(1024)}, u32[]{:S(2)}) copy-start(f32[2048]{0:T(1024)} %param.9) | copy-start | bytes 24580
